TPU v7x, 32 devices: a whole 2x2x4 slice. The times are simulated.
32 devices in a mesh: ep: 8 (over z, core), tp: 4 (over y, x).
Axes of the slice: x: 2, y: 2, z: 4, core: 2. Of those that a mesh axis runs over, the one named last changes fastest.
Arguments:
- pool_input: bfloat16 [2048, 2048], P('ep'), may hold values from -6 to 6
- pool_gain: float32 [2048], replicated, may hold values from 0.1 to 1.9
- pool_weight: bfloat16 [512, 2048], P(None, 'tp'), may hold values from -0.25 to 0.25
- pool_scale: float32 [2048], P('tp'), may hold values from 0.1 to 1.9
- moe_input: bfloat16 [1536, 2048], P('ep'), may hold values from -6 to 6
- moe_gain: float32 [2048], replicated, may hold values from 0.1 to 1.9
- routes: int32 [1536, 2], P('ep'), may hold values from 0 to 7, all different within a row; in each aligned block of 192 rows (0 to 191, 192 to 383, ...) at most 96 rows name the same one
- route_logits: float32 [1536, 2], P('ep'), may hold values from -4 to 4
- gate_weight: bfloat16 [8, 2048, 4096], P('ep', None, 'tp'), may hold values from -0.125 to 0.125
- up_weight: bfloat16 [8, 2048, 4096], P('ep', None, 'tp'), may hold values from -0.125 to 0.125
- down_weight: bfloat16 [8, 2048, 4096], P('ep', None, 'tp'), may hold values from -0.09375 to 0.09375
Outputs:
- pool_out: bfloat16 [2048, 2048], P('ep', 'tp')
- expert_out: bfloat16 [1536, 2048], P('ep', 'tp')
Inputs may be any that keep to these rules, and one draw needn't show every extreme that they name: `routes`: the 2 experts of a token differ. Within the rows of one device (aligned blocks of 192 rows) no expert is named by more than 96 rows, and in every draw some expert is named by exactly 96 rows of some device.
All inputs are finite; a program needn't handle non-finite values.
Results may differ from a plain program's by a relative error of at most 0.017.
Values may be sent and summed in bfloat16 or wider, within the bound.
A program may use at most 64 MiB of HBM per device.

v0:
```python
import jax
import jax.numpy as jnp
from jax import lax
from jax.sharding import PartitionSpec as P

GROUP_WIDTH = 512


EPSILON = 1e-06
halo_rows = 15


def passed_along(value, axis, steps):
    count = lax.axis_size(axis)
    leading, last = (max(0, -steps), min(count, count - steps))
    return lax.ppermute(value, axis, [(source, source + steps) for source in range(leading, last)])


def rms_rows(row_block, scale_gain):
    values = row_block.astype(jnp.float32)
    scaled = values * lax.rsqrt(jnp.mean(values * values, axis=-1, keepdims=True) + EPSILON)
    return (scaled * scale_gain).astype(jnp.bfloat16)


def delayed(values, offset):
    return jnp.concatenate(
        [jnp.zeros((offset,) + values.shape[1:], values.dtype), values[:-offset]], axis=0
    )


def window_sums(values):
    totals = []
    current = values
    for offset in (1, 2, 4, 8):
        current = current + delayed(current, offset)
        totals.append(current)
    return totals


def slot_tables(route_block, expert_count, capacity):
    tokens_count = route_block.shape[0]
    picks_count = route_block.shape[1]
    flat_ids = route_block.reshape(-1)
    onehot = (flat_ids[:, None] == jnp.arange(expert_count, dtype=jnp.int32)[None, :]).astype(
        jnp.int32
    )
    before = jnp.cumsum(onehot, axis=0) - onehot
    rank_in = jnp.sum(before * onehot, axis=1)
    slot_ids = flat_ids * capacity + rank_in
    owners = jnp.repeat(jnp.arange(tokens_count, dtype=jnp.int32), picks_count)
    holder = jnp.full((expert_count * capacity,), tokens_count, jnp.int32).at[slot_ids].set(owners)
    return (slot_ids, holder)


def pool_half(pool_input, pool_gain, pool_weight, pool_scale):
    normed = rms_rows(pool_input, pool_gain)
    local_rows = normed.shape[0]
    column_count = pool_weight.shape[1]
    group_index = lax.axis_index("tp") * column_count // GROUP_WIDTH
    own_group = lax.dynamic_slice_in_dim(normed, group_index * GROUP_WIDTH, GROUP_WIDTH, 1)
    earlier = passed_along(own_group[local_rows - halo_rows :], "ep", 1)
    extended = jnp.concatenate([earlier, own_group], axis=0).astype(jnp.float32)
    stacked = jnp.stack(window_sums(extended))[:, halo_rows:]
    chosen = lax.dynamic_index_in_dim(stacked, group_index, 0, keepdims=False)
    position = lax.axis_index("ep") * local_rows + lax.iota(jnp.int32, local_rows)
    window = jnp.left_shift(jnp.int32(2), group_index)
    counts = jnp.minimum(position + 1, window).astype(jnp.float32)
    mixed_in = (chosen / counts[:, None] - own_group.astype(jnp.float32)).astype(jnp.bfloat16)
    product = jnp.dot(mixed_in, pool_weight, preferred_element_type=jnp.float32)
    return (product * pool_scale).astype(jnp.bfloat16)


def expert_half(moe_input, moe_gain, routes, route_logits, gate_weight, up_weight, down_weight):
    normed = rms_rows(moe_input, moe_gain)
    local_rows, row_width = normed.shape
    picks_count = routes.shape[1]
    experts = lax.axis_size("ep")
    capacity = 2 * local_rows * picks_count // experts
    slot_ids, holder = slot_tables(routes, experts, capacity)
    padded = jnp.concatenate([normed, jnp.zeros((1, row_width), jnp.bfloat16)], axis=0)
    gate_block = gate_weight[0]
    up_block = up_weight[0]
    down_block = down_weight[0]
    column_count = row_width // lax.axis_size("tp")
    start_col = lax.axis_index("tp") * column_count
    narrow = lax.dynamic_slice_in_dim(padded, start_col, column_count, 1)
    outgoing = narrow[holder].reshape(experts, capacity, column_count)
    arrived = lax.all_to_all(outgoing, "ep", split_axis=0, concat_axis=0, tiled=True).reshape(
        experts * capacity, column_count
    )
    segment = lax.all_gather(arrived, "tp", axis=1, tiled=True)
    gate_part = jnp.dot(segment, gate_block, preferred_element_type=jnp.float32)
    up_part = jnp.dot(segment, up_block, preferred_element_type=jnp.float32)
    hidden = (jax.nn.silu(gate_part) * up_part).astype(jnp.bfloat16)
    summed = lax.psum_scatter(
        lax.dot_general(
            down_block, hidden, (((1,), (1,)), ((), ())), preferred_element_type=jnp.float32
        ).astype(jnp.bfloat16),
        "tp",
        scatter_dimension=0,
        tiled=True,
    ).astype(jnp.float32)
    results = summed.astype(jnp.bfloat16).reshape(summed.shape[0], experts, capacity)
    returned = lax.all_to_all(results, "ep", split_axis=1, concat_axis=1, tiled=True).reshape(
        summed.shape[0], experts * capacity
    )
    picked = (
        returned[:, slot_ids].astype(jnp.float32).reshape(summed.shape[0], local_rows, picks_count)
    )
    raised = jnp.exp(route_logits)
    shares = raised / jnp.sum(raised, axis=-1, keepdims=True)
    combined = jnp.einsum("dtk,tk->td", picked, shares)
    return combined.astype(jnp.bfloat16)


def local(
    pool_input,
    pool_gain,
    pool_weight,
    pool_scale,
    moe_input,
    moe_gain,
    routes,
    route_logits,
    gate_weight,
    up_weight,
    down_weight,
):
    pool_out = pool_half(pool_input, pool_gain, pool_weight, pool_scale)
    expert_out = expert_half(
        moe_input, moe_gain, routes, route_logits, gate_weight, up_weight, down_weight
    )
    return (pool_out, expert_out)


def solution(mesh):
    in_specs = (
        P("ep", None),
        P(),
        P(None, "tp"),
        P("tp"),
        P("ep", None),
        P(),
        P("ep", None),
        P("ep", None),
        P("ep", None, "tp"),
        P("ep", None, "tp"),
        P("ep", None, "tp"),
    )
    out_specs = (P("ep", "tp"), P("ep", "tp"))
    return jax.shard_map(local, mesh=mesh, in_specs=in_specs, out_specs=out_specs, check_vma=False)
```

profile of v0, /device:TPU:0, one launch (start us, length us, event | category | flops | bytes accessed | tf_op | source)
XLA Modules:
  0.0 184.2 jit_solution(8326187543108541298)
XLA Ops:
  7.2 0.0 copy-start
  7.2 0.0 all-gather.2.cloned.1.call-start
  7.2 0.8 copy.14
  8.1 0.1 eq.29
  8.2 0.1 eq.25
  8.4 0.7 broadcast_multiply_fusion
  9.1 1.4 fusion.14
  10.4 0.9 reduce-window.6
  11.3 0.2 slice_reduce_fusion
  11.6 0.1 copy.13
  11.7 0.1 mul.99
  11.9 0.1 reshape.122
  12.0 0.1 fusion.29
  12.1 2.9 %scatter_custom_fusion = s32[768]{0:T(1024)S(1)} fusion(s32[384]{0:T(512)S(1)} %fusion.33, s32[384]{0:T(512)S(1)} %reshape.122, s32[]{:T(128)} %constant.67.clone.1), kind=kCustom, calls=%fused_computation.53 | custom fusion | bytes 3076 | tf_op jit(solution)/shard_map/scatter | solution.py:51
  15.1 1.4 fusion.16
  16.5 2.7 %gather_fusion = bf16[768,512]{1,0:T(8,128)(2,1)S(1)} fusion(bf16[193,512]{1,0:T(8,128)(2,1)S(1)} %pad_dynamic-slice_fusion.4, s32[1024]{0:T(1024)S(1)} %pad_clamp_fusion.1), kind=kCustom, calls=%fused_computation | custom fusion | bytes 1575936 | tf_op jit(solution)/shard_map/gather | solution.py:87
  19.2 27.2 %all_to_all.10 = bf16[8,96,512]{2,1,0:T(8,128)(2,1)} all-to-all(bf16[8,96,512]{2,1,0:T(8,128)(2,1)S(1)} %bitcast.67), channel_id=1, replica_groups=mesh['ep'=8,'tp'=4] {'ep'}, dimensions={0} | all-to-all | bytes 1572864 | tf_op jit(solution)/shard_map/all_to_all | solution.py:88
  46.4 0.0 all-gather.2.cloned.1.call-update
  46.4 0.0 reduce-scatter.2.cloned.1.call-start
  46.5 42.8 %all-gather.2.cloned.1.call-done = bf16[768,2048]{1,0:T(8,128)(2,1)} async-done(((bf16[768,512]{1,0:T(8,128)(2,1)}), bf16[768,2048]{1,0:T(8,128)(2,1)}) %all-gather.2.cloned.1.call-update) | async-done | bytes 3145744 | tf_op jit(solution)/shard_map/all_gather | solution.py:91
  89.2 6.3 %fusion.2 = f32[768,1024]{1,0:T(8,128)S(1)} fusion(bf16[768,2048]{1,0:T(8,128)(2,1)} %all-gather.2.cloned.1.call-done, bf16[1,2048,1024]{2,1,0:T(8,128)(2,1)} %param.20), kind=kOutput, calls=%fused_computation.5 | convolution fusion | flops 3221225472 | bytes 10485760 | tf_op jit(solution)/shard_map/dot_general | solution.py:93
  95.5 0.0 copy-start.4
  95.5 3.8 %multiply_convert_fusion = bf16[768,1024]{1,0:T(8,128)(2,1)S(1)} fusion(f32[768,1024]{1,0:T(8,128)S(1)} %fusion.2, bf16[768,2048]{1,0:T(8,128)(2,1)S(1)} %copy-done.5, bf16[1,2048,1024]{2,1,0:T(8,128)(2,1)S(1)} %copy-done.3), kind=kOutput, calls=%fused_computation.10 | convolution fusion | flops 3225944064 | bytes 12058624 | tf_op jit(solution)/shard_map/dot_general | solution.py:92
  99.4 4.9 %fusion.9 = bf16[2048,768]{0,1:T(8,128)(2,1)} fusion(bf16[768,1024]{1,0:T(8,128)(2,1)S(1)} %multiply_convert_fusion, bf16[1,2048,1024]{2,1,0:T(8,128)(2,1)S(1)} %copy-done.4), kind=kOutput, calls=%fused_computation.11 | convolution fusion | flops 3222798336 | bytes 8912896 | tf_op jit(solution)/shard_map/dot_general | solution.py:96
  104.3 0.0 reduce-scatter.2.cloned.1.call-update
  104.3 0.0 copy-start.2
  104.3 1.2 copy-done.1
  105.5 1.6 convert_element_type.53
  107.1 0.8 dynamic-slice
  107.9 0.3 multiply_reduce_fusion
  108.1 1.2 fusion.25
  109.3 1.6 collective-permute-start
  111.0 37.4 %reduce-scatter.2.cloned.1.call-done = bf16[512,768]{0,1:T(8,128)(2,1)} async-done(((bf16[2048,768]{0,1:T(8,128)(2,1)}), bf16[512,768]{0,1:T(8,128)(2,1)}) %reduce-scatter.2.cloned.1.call-update) | async-done | bytes 786448 | tf_op jit(solution)/shard_map/reduce_scatter | solution.py:95
  148.3 4.6 %all-to-all-start.1 = ((bf16[512,8,96]{0,2,1:T(8,128)(2,1)}), bf16[512,8,96]{0,2,1:T(8,128)(2,1)S(1)}, u32[]{:S(2)}, u32[]{:S(2)}) async-start(bf16[512,8,96]{0,2,1:T(8,128)(2,1)} %bitcast.71), calls=%async_computation.2 | async-start | bytes 1572864 | tf_op jit(solution)/shard_map/all_to_all | solution.py:104
  153.0 0.2 copy.16
  153.2 0.1 maximum_convert_fusion
  153.3 0.1 pad_add_fusion.2
  153.4 0.0 copy-start.6
  153.4 0.1 pad_add_fusion.1
  153.5 0.1 pad_add_fusion
  153.7 0.1 add_bitcast_fusion
  153.8 0.3 copy-done.6
  154.1 1.2 fusion.17
  155.3 18.6 %all-to-all-done.1 = bf16[512,8,96]{0,2,1:T(8,128)(2,1)S(1)} async-done(((bf16[512,8,96]{0,2,1:T(8,128)(2,1)}), bf16[512,8,96]{0,2,1:T(8,128)(2,1)S(1)}, u32[]{:S(2)}, u32[]{:S(2)}) %all-to-all-start.1) | async-done | bytes 786464 | tf_op jit(solution)/shard_map/all_to_all | solution.py:104
  173.9 2.1 %gather_fusion.1 = bf16[384,512]{1,0:T(8,128)(2,1)S(1)} fusion(bf16[512,768]{0,1:T(8,128)(2,1)S(1)} %bitcast.61, s32[1024]{0:T(1024)S(1)} %pad_clamp_fusion), kind=kCustom, calls=%fused_computation.1 | custom fusion | bytes 787968 | tf_op jit(solution)/shard_map/gather | solution.py:108
  176.0 0.2 reshape.101
  176.1 0.6 fusion.36
  176.7 0.7 copy.19
  (24 shorter events, 0.2 us)
Async XLA Ops:
  7.2 146.6 %copy-start = (bf16[512,512]{1,0:T(8,128)(2,1)S(1)}, bf16[512,512]{1,0:T(8,128)(2,1)}, u32[]{:S(2)}) copy-start(bf16[512,512]{1,0:T(8,128)(2,1)} %param.13) | copy-start | bytes 1572868
  7.2 82.0 %all-gather.2.cloned.1.call-start = ((), (), s32[]{:S(2)}) async-start(), calls=%async_computation.3 | async-start | bytes 3932160 | tf_op jit(solution)/shard_map/all_gather | solution.py:91
  46.4 101.9 %reduce-scatter.2.cloned.1.call-start = ((), (), s32[]{:S(2)}) async-start(), calls=%async_computation.4 | async-start | bytes 3932160 | tf_op jit(solution)/shard_map/reduce_scatter | solution.py:95
  89.2 6.3 %copy-start.3 = (bf16[1,2048,1024]{2,1,0:T(8,128)(2,1)S(1)}, bf16[1,2048,1024]{2,1,0:T(8,128)(2,1)}, u32[]{:S(2)}) copy-start(bf16[1,2048,1024]{2,1,0:T(8,128)(2,1)} %param.19) | copy-start | bytes 12582916
  89.2 6.3 %copy-start.5 = (bf16[768,2048]{1,0:T(8,128)(2,1)S(1)}, bf16[768,2048]{1,0:T(8,128)(2,1)}, u32[]{:S(2)}) copy-start(bf16[768,2048]{1,0:T(8,128)(2,1)} %all-gather.2.cloned.1.call-done) | copy-start | bytes 9437188
  95.5 3.8 %copy-start.4 = (bf16[1,2048,1024]{2,1,0:T(8,128)(2,1)S(1)}, bf16[1,2048,1024]{2,1,0:T(8,128)(2,1)}, u32[]{:S(2)}) copy-start(bf16[1,2048,1024]{2,1,0:T(8,128)(2,1)} %param.21) | copy-start | bytes 12582916
  104.3 1.2 copy-start.1
  104.3 6.6 %copy-start.2 = (f32[192,2]{0,1:T(2,128)S(1)}, f32[192,2]{0,1:T(2,128)}, u32[]{:S(2)}) copy-start(f32[192,2]{0,1:T(2,128)} %param.18) | copy-start | bytes 4612
  109.3 43.8 %collective-permute-start = (bf16[15,512]{1,0:T(8,128)(2,1)S(1)}, bf16[15,512]{1,0:T(8,128)(2,1)S(1)}, u32[]{:S(2)}, u32[]{:S(2)}) collective-permute-start(bf16[15,512]{1,0:T(8,128)(2,1)S(1)} %slice.36), channel_id=1, source_target_pairs={{0,4},{4,8},{8,12},{12,16},{16,20},{20,24},{24,28},{1,5},{5,9},{9,... | collective-permute-start | bytes 46088 | tf_op jit(solution)/shard_map/ppermute | solution.py:16
  148.3 25.6 %all-to-all-start.1 = ((bf16[512,8,96]{0,2,1:T(8,128)(2,1)}), bf16[512,8,96]{0,2,1:T(8,128)(2,1)S(1)}, u32[]{:S(2)}, u32[]{:S(2)}) async-start(bf16[512,8,96]{0,2,1:T(8,128)(2,1)} %bitcast.71), calls=%async_computation.2 | async-start | bytes 1572864 | tf_op jit(solution)/shard_map/all_to_all | solution.py:104
  153.4 0.7 copy-start.6
Sparse Core Ops, SparseCore 0:
  46.5 42.6 all-gather.1
  104.4 43.8 reduce-scatter.1
where the time goes:
time: 185 us; the launch traced here: 184 us
  waiting for transfers between devices  98.8 us (53%)
  blocking collectives  27.2 us (15%)
  matrix products  16.7 us (9%)
  between operations  14.4 us (8%)
  local copies, waits for them, and re-layouts  12.8 us (7%)
  other arithmetic  8.08 us (4%)
  starting transfers between devices  6.26 us (3%)
    all_gather x1, waiting for transfers between devices, expert_half(): segment = lax.all_gather(arrived, 'tp', axis=1, tiled=True)  42.8 us
    reduce_scatter x1, waiting for transfers between devices, expert_half(): lax.psum_scatter(lax.dot_general(down_block, hidden, (((1,), (1,)), ((),...  37.4 us
    all_to_all x1, blocking collectives, expert_half(): lax.all_to_all(outgoing, 'ep', split_axis=0, concat_axis=0, tiled=True)  27.2 us
    all_to_all x1, waiting for transfers between devices, expert_half(): lax.all_to_all(results, 'ep', split_axis=1, concat_axis=1, tiled=True)  18.6 us
    dot_general x1, matrix products, expert_half(): up_part = jnp.dot(segment, up_block, preferred_element_type=jnp.float32)  6.28 us
    dot_general x1, matrix products, expert_half(): lax.dot_general(down_block, hidden, (((1,), (1,)), ((), ())), preferred_e...  4.88 us
    all_to_all x1, starting transfers between devices, expert_half(): lax.all_to_all(results, 'ep', split_axis=1, concat_axis=1, tiled=True)  4.61 us
    dot_general x1, matrix products, expert_half(): gate_part = jnp.dot(segment, gate_block, preferred_element_type=jnp.float32)  3.82 us
  transfers between devices with their start and end apart: 4, of which 3 were waited for; matrix products, arithmetic and copies ran while one was open for 3% of the time, Pallas kernels for 0%

commit v1 on v0

v1 whole, which is shorter than its diff:
```python
import functools

import jax
import jax.numpy as jnp
from jax import lax
from jax.experimental import pallas as pl
from jax.experimental.pallas import tpu as pltpu
from jax.sharding import PartitionSpec as P

GROUP_WIDTH = 512


EPSILON = 1e-06
halo_rows = 15


def passed_along(value, axis, steps):
    count = lax.axis_size(axis)
    leading, last = (max(0, -steps), min(count, count - steps))
    return lax.ppermute(value, axis, [(source, source + steps) for source in range(leading, last)])


def rms_rows(row_block, scale_gain):
    values = row_block.astype(jnp.float32)
    scaled = values * lax.rsqrt(jnp.mean(values * values, axis=-1, keepdims=True) + EPSILON)
    return (scaled * scale_gain).astype(jnp.bfloat16)


def delayed(values, offset):
    return jnp.concatenate(
        [jnp.zeros((offset,) + values.shape[1:], values.dtype), values[:-offset]], axis=0
    )


def window_sums(values):
    totals = []
    current = values
    for offset in (1, 2, 4, 8):
        current = current + delayed(current, offset)
        totals.append(current)
    return totals


def pool_half(pool_input, pool_gain, pool_weight, pool_scale):
    normed = rms_rows(pool_input, pool_gain)
    local_rows = normed.shape[0]
    column_count = pool_weight.shape[1]
    group_index = lax.axis_index("tp") * column_count // GROUP_WIDTH
    own_group = lax.dynamic_slice_in_dim(normed, group_index * GROUP_WIDTH, GROUP_WIDTH, 1)
    earlier = passed_along(own_group[local_rows - halo_rows :], "ep", 1)
    extended = jnp.concatenate([earlier, own_group], axis=0).astype(jnp.float32)
    stacked = jnp.stack(window_sums(extended))[:, halo_rows:]
    chosen = lax.dynamic_index_in_dim(stacked, group_index, 0, keepdims=False)
    position = lax.axis_index("ep") * local_rows + lax.iota(jnp.int32, local_rows)
    window = jnp.left_shift(jnp.int32(2), group_index)
    counts = jnp.minimum(position + 1, window).astype(jnp.float32)
    mixed_in = (chosen / counts[:, None] - own_group.astype(jnp.float32)).astype(jnp.bfloat16)
    product = jnp.dot(mixed_in, pool_weight, preferred_element_type=jnp.float32)
    return (product * pool_scale).astype(jnp.bfloat16)


def expert_kernel(
    sizes,
    tokens_ref,
    gain_ref,
    select_ref,
    blend_ref,
    gate_hbm,
    up_hbm,
    down_hbm,
    out_ref,
    normed,
    outgoing,
    sibling_out,
    rows_in,
    parts,
    first_in0,
    first_in1,
    half_sum0,
    half_sum1,
    second_in0,
    second_in1,
    finished,
    returned,
    gate_ref,
    up_ref,
    down_ref,
    weight_sem,
    go_send,
    go_recv,
    a0_send,
    a0_recv,
    a1_send,
    a1_recv,
    b0_send,
    b0_recv,
    b1_send,
    b1_recv,
    ra0_send,
    ra0_recv,
    ra1_send,
    ra1_recv,
    rb0_send,
    rb0_recv,
    rb1_send,
    rb1_recv,
    back_send,
    back_recv,
):
    experts, ny, nx, slots, columns = sizes
    pairs = experts // 2
    me, shard = lax.axis_index("ep"), lax.axis_index("tp")
    my_pair, my_core = me // 2, me % 2
    my_y, my_x = shard // nx, shard % nx
    bf16, f32 = jnp.bfloat16, jnp.float32
    pending = []

    def device_at(ep, y, x):
        return {"ep": ep, "tp": y * nx + x}

    def copy_to(src, dst, send, recv, target):
        return pltpu.make_async_remote_copy(
            src_ref=src,
            dst_ref=dst,
            send_sem=send,
            recv_sem=recv,
            device_id=target,
            device_id_type=pl.DeviceIdType.MESH,
        )

    def start(*arguments):
        copy = copy_to(*arguments)
        copy.start()
        pending.append(copy)

    def arrive(ref, send, recv):
        copy_to(ref, ref, send, recv, device_at(me, my_y, my_x)).wait_recv()

    weight_copies = [
        pltpu.make_async_copy(source.at[0], target, weight_sem.at[number])
        for number, (source, target) in enumerate(
            ((gate_hbm, gate_ref), (up_hbm, up_ref), (down_hbm, down_ref))
        )
    ]
    for copy in weight_copies:
        copy.start()

    others_x = [lax.rem(my_x + step, nx) for step in range(1, nx)]
    others_y = [lax.rem(my_y + step, ny) for step in range(1, ny)]
    barrier = pltpu.get_barrier_semaphore()
    greeted = [device_at(lax.rem(me + step, experts), my_y, my_x) for step in range(1, experts)]
    greeted += [device_at(me, my_y, x) for x in others_x]
    greeted += [device_at(me, y, my_x) for y in others_y]
    for target in greeted:
        pl.semaphore_signal(
            barrier, inc=1, device_id=target, device_id_type=pl.DeviceIdType.MESH
        )

    values = tokens_ref[...].astype(f32)
    scale = lax.rsqrt(jnp.mean(values * values, axis=-1, keepdims=True) + EPSILON)
    normed[...] = (values * scale * gain_ref[...]).astype(bf16)
    own_columns = pl.ds(pl.multiple_of(shard * columns, columns), columns)
    narrow = normed[:, own_columns]

    def pair_at(step):
        return lax.rem(my_pair + step, pairs)

    for step in range(1, pairs):
        target_pair = lax.rem(my_pair + pairs - step, pairs)
        for core in range(2):
            expert = target_pair * 2 + core
            outgoing[expert] = jnp.dot(
                select_ref[expert], narrow, preferred_element_type=f32
            ).astype(bf16)
    sibling = my_pair * 2 + 1 - my_core
    wide = normed[...]
    for_sibling = jnp.dot(select_ref[sibling], wide, preferred_element_type=f32).astype(bf16)
    for_self = jnp.dot(select_ref[me], wide, preferred_element_type=f32).astype(bf16)
    my_rows = pl.ds(pl.multiple_of(my_core * slots, slots), slots)
    for y in range(ny):
        for x in range(nx):
            begin = (y * nx + x) * columns
            sibling_out[y, x] = for_sibling[:, begin : begin + columns]
            rows_in[my_pair, y, x, my_rows, :] = for_self[:, begin : begin + columns]
    pl.semaphore_wait(barrier, len(greeted))

    start(
        sibling_out,
        rows_in.at[my_pair, :, :, my_rows],
        go_send.at[sibling],
        go_recv.at[me],
        device_at(sibling, my_y, my_x),
    )
    for step in range(1, pairs):
        target_pair = lax.rem(my_pair + pairs - step, pairs)
        for core in range(2):
            expert = target_pair * 2 + core
            start(
                outgoing.at[expert],
                rows_in.at[my_pair, my_y, my_x, my_rows],
                go_send.at[expert],
                go_recv.at[me],
                device_at(expert, my_y, my_x),
            )

    def rows_of(core):
        return pl.ds(core * slots, slots)

    def spread_first(step):
        pair = pair_at(step)
        for core in range(2):
            block = rows_in.at[pair, my_y, my_x, rows_of(core)]
            source = pair * 2 + core
            arrive(block, go_send.at[source], go_recv.at[source])
            if core == 0:
                for x in others_x:
                    start(block, block, a0_send.at[pair, x], a0_recv.at[pair, my_x], device_at(me, my_y, x))
            else:
                for y in others_y:
                    start(block, block, a1_send.at[pair, y], a1_recv.at[pair, my_y], device_at(me, y, my_x))

    def spread_second(step):
        pair = pair_at(step)
        for x in others_x:
            arrive(rows_in.at[pair, my_y, x, rows_of(0)], a0_send.at[pair, x], a0_recv.at[pair, x])
        held = rows_in.at[pair, my_y, :, rows_of(0)]
        for y in others_y:
            start(held, held, b0_send.at[pair, y], b0_recv.at[pair, my_y], device_at(me, y, my_x))
        for y in others_y:
            arrive(rows_in.at[pair, y, my_x, rows_of(1)], a1_send.at[pair, y], a1_recv.at[pair, y])
        held = rows_in.at[pair, :, my_x, rows_of(1)]
        for x in others_x:
            start(held, held, b1_send.at[pair, x], b1_recv.at[pair, my_x], device_at(me, my_y, x))

    def spread_end(step):
        pair = pair_at(step)
        for y in others_y:
            arrive(rows_in.at[pair, y, :, rows_of(0)], b0_send.at[pair, y], b0_recv.at[pair, y])
        for x in others_x:
            arrive(rows_in.at[pair, :, x, rows_of(1)], b1_send.at[pair, x], b1_recv.at[pair, x])

    def multiply(step):
        pair = pair_at(step)
        entire = jnp.concatenate(
            [rows_in[pair, y, x] for y in range(ny) for x in range(nx)], axis=1
        )
        gate_part = jnp.dot(entire, gate_ref[...], preferred_element_type=f32)
        up_part = jnp.dot(entire, up_ref[...], preferred_element_type=f32)
        hidden = (gate_part / (1.0 + jnp.exp(-gate_part)) * up_part).astype(bf16)
        for y in range(ny):
            for x in range(nx):
                begin = (y * nx + x) * columns
                parts[pair, y, x] = lax.dot_general(
                    hidden,
                    down_ref[begin : begin + columns, :],
                    (((1,), (1,)), ((), ())),
                    preferred_element_type=f32,
                ).astype(bf16)
        for x in others_x:
            start(
                parts.at[pair, :, x, rows_of(0)],
                first_in0.at[pair, my_x],
                ra0_send.at[pair, x],
                ra0_recv.at[pair, my_x],
                device_at(me, my_y, x),
            )
        for y in others_y:
            start(
                parts.at[pair, y, :, rows_of(1)],
                first_in1.at[pair, my_y],
                ra1_send.at[pair, y],
                ra1_recv.at[pair, my_y],
                device_at(me, y, my_x),
            )

    def reduce_first(step):
        pair = pair_at(step)
        for x in others_x:
            arrive(first_in0.at[pair, x], ra0_send.at[pair, x], ra0_recv.at[pair, x])
        for y in range(ny):
            total = parts[pair, y, my_x, rows_of(0), :].astype(f32)
            for x in others_x:
                total += first_in0[pair, x, y].astype(f32)
            half_sum0[pair, y] = total.astype(bf16)
        for y in others_y:
            start(
                half_sum0.at[pair, y],
                second_in0.at[pair, my_y],
                rb0_send.at[pair, y],
                rb0_recv.at[pair, my_y],
                device_at(me, y, my_x),
            )
        for y in others_y:
            arrive(first_in1.at[pair, y], ra1_send.at[pair, y], ra1_recv.at[pair, y])
        for x in range(nx):
            total = parts[pair, my_y, x, rows_of(1), :].astype(f32)
            for y in others_y:
                total += first_in1[pair, y, x].astype(f32)
            half_sum1[pair, x] = total.astype(bf16)
        for x in others_x:
            start(
                half_sum1.at[pair, x],
                second_in1.at[pair, my_x],
                rb1_send.at[pair, x],
                rb1_recv.at[pair, my_x],
                device_at(me, my_y, x),
            )

    def reduce_second(step):
        pair = pair_at(step)
        for y in others_y:
            arrive(second_in0.at[pair, y], rb0_send.at[pair, y], rb0_recv.at[pair, y])
        total = half_sum0[pair, my_y].astype(f32)
        for y in others_y:
            total += second_in0[pair, y].astype(f32)
        finished[pair * 2] = total.astype(bf16)
        for x in others_x:
            arrive(second_in1.at[pair, x], rb1_send.at[pair, x], rb1_recv.at[pair, x])
        total = half_sum1[pair, my_x].astype(f32)
        for x in others_x:
            total += second_in1[pair, x].astype(f32)
        finished[pair * 2 + 1] = total.astype(bf16)
        if step == 0:
            targets = [sibling]
            returned[me] = finished[me]
        else:
            targets = [pair * 2, pair * 2 + 1]
        for target in targets:
            start(
                finished.at[target],
                returned.at[me],
                back_send.at[target],
                back_recv.at[me],
                device_at(target, my_y, my_x),
            )

    arrive(
        rows_in.at[my_pair, :, :, pl.ds(pl.multiple_of((1 - my_core) * slots, slots), slots)],
        go_send.at[sibling],
        go_recv.at[sibling],
    )
    for copy in weight_copies:
        copy.wait()
    multiply(0)
    for turn in range(1, pairs + 4):
        if turn < pairs:
            spread_first(turn)
        if 1 <= turn - 1 < pairs:
            spread_second(turn - 1)
        if 1 <= turn - 2 < pairs:
            spread_end(turn - 2)
            multiply(turn - 2)
        if 0 <= turn - 3 < pairs:
            reduce_first(turn - 3)
        if 0 <= turn - 4 < pairs:
            reduce_second(turn - 4)
    total = jnp.dot(blend_ref[me], returned[me], preferred_element_type=f32)
    for step in range(1, experts):
        source = lax.rem(me + step, experts)
        arrive(returned.at[source], back_send.at[source], back_recv.at[source])
        total += jnp.dot(blend_ref[source], returned[source], preferred_element_type=f32)
    out_ref[...] = total.astype(bf16)
    for copy in pending:
        copy.wait_send()


def expert_half(moe_input, moe_gain, routes, route_logits, gate_weight, up_weight, down_weight):
    local_rows, row_width = moe_input.shape
    picks_count = routes.shape[1]
    experts, shards = lax.axis_size("ep"), lax.axis_size("tp")
    capacity = 2 * local_rows * picks_count // experts
    slots = -(-capacity // 16) * 16
    columns = row_width // shards
    ny = max(d for d in range(1, shards + 1) if shards % d == 0 and d * d <= shards)
    nx = shards // ny
    pairs = experts // 2
    hidden_units = gate_weight.shape[2]

    expert_ids = jnp.arange(experts, dtype=jnp.int32)
    named = (routes[:, :, None] == expert_ids).astype(jnp.float32)
    visits = jnp.sum(named, axis=1)
    order = jnp.arange(local_rows, dtype=jnp.int32)
    earlier = (order[:, None] > order[None, :]).astype(jnp.float32)
    rank = jnp.dot(earlier, visits, preferred_element_type=jnp.float32).astype(jnp.int32)
    raised = jnp.exp(route_logits)
    shares = raised / jnp.sum(raised, axis=-1, keepdims=True)
    share_of = jnp.sum(named * shares[:, :, None], axis=1)
    slot_ids = jnp.arange(slots, dtype=jnp.int32)
    rank_of, visits_of = rank.T, visits.T
    select = jnp.where(
        rank_of[:, None, :] == slot_ids[None, :, None], visits_of[:, None, :], 0.0
    ).astype(jnp.bfloat16)
    blend = jnp.where(
        rank_of[:, :, None] == slot_ids[None, None, :], share_of.T[:, :, None], 0.0
    ).astype(jnp.bfloat16)

    bf16 = jnp.bfloat16
    dma = pltpu.SemaphoreType.DMA
    vmem = pl.BlockSpec(memory_space=pltpu.VMEM)
    anywhere = pl.BlockSpec(memory_space=pl.ANY)
    block = (slots, columns)
    sems_x, sems_y = dma((pairs, nx)), dma((pairs, ny))
    return pl.pallas_call(
        functools.partial(expert_kernel, (experts, ny, nx, slots, columns)),
        out_shape=jax.ShapeDtypeStruct((local_rows, columns), bf16),
        in_specs=[vmem] * 4 + [anywhere] * 3,
        out_specs=vmem,
        scratch_shapes=[
            pltpu.VMEM((local_rows, row_width), bf16),
            pltpu.VMEM((experts,) + block, bf16),
            pltpu.VMEM((ny, nx) + block, bf16),
            pltpu.VMEM((pairs, ny, nx, 2 * slots, columns), bf16),
            pltpu.VMEM((pairs, ny, nx, 2 * slots, columns), bf16),
            pltpu.VMEM((pairs, nx, ny) + block, bf16),
            pltpu.VMEM((pairs, ny, nx) + block, bf16),
            pltpu.VMEM((pairs, ny) + block, bf16),
            pltpu.VMEM((pairs, nx) + block, bf16),
            pltpu.VMEM((pairs, ny) + block, bf16),
            pltpu.VMEM((pairs, nx) + block, bf16),
            pltpu.VMEM((experts,) + block, bf16),
            pltpu.VMEM((experts,) + block, bf16),
            pltpu.VMEM((row_width, hidden_units), bf16),
            pltpu.VMEM((row_width, hidden_units), bf16),
            pltpu.VMEM((row_width, hidden_units), bf16),
            dma((3,)),
            dma((experts,)),
            dma((experts,)),
        ]
        + [sems_x, sems_x, sems_y, sems_y, sems_y, sems_y, sems_x, sems_x] * 2
        + [dma((experts,)), dma((experts,))],
        compiler_params=pltpu.CompilerParams(
            collective_id=0, has_side_effects=True, vmem_limit_bytes=58 * 1024 * 1024
        ),
    )(
        moe_input,
        moe_gain.reshape(1, row_width),
        select,
        blend,
        gate_weight,
        up_weight,
        down_weight,
    )


def local(
    pool_input,
    pool_gain,
    pool_weight,
    pool_scale,
    moe_input,
    moe_gain,
    routes,
    route_logits,
    gate_weight,
    up_weight,
    down_weight,
):
    pool_out = pool_half(pool_input, pool_gain, pool_weight, pool_scale)
    expert_out = expert_half(
        moe_input, moe_gain, routes, route_logits, gate_weight, up_weight, down_weight
    )
    return (pool_out, expert_out)


def solution(mesh):
    in_specs = (
        P("ep", None),
        P(),
        P(None, "tp"),
        P("tp"),
        P("ep", None),
        P(),
        P("ep", None),
        P("ep", None),
        P("ep", None, "tp"),
        P("ep", None, "tp"),
        P("ep", None, "tp"),
    )
    out_specs = (P("ep", "tp"), P("ep", "tp"))
    return jax.shard_map(local, mesh=mesh, in_specs=in_specs, out_specs=out_specs, check_vma=False)
```

time: 185 us -> 86.9 us (0.47)
  waiting for transfers between devices: 98.8 us -> 0.01 us
  Pallas kernels: 0 us -> 72.3 us
  blocking collectives: 27.2 us -> 0 us
  matrix products: 16.7 us -> 1.35 us
  between operations: 14.4 us -> 0.85 us
  local copies, waits for them, and re-layouts: 12.8 us -> 1.93 us
  starting transfers between devices: 6.26 us -> 2.4 us
    pallas_call x0 -> x1, Pallas kernels: none -> 72.3 us  [expert_half(): pl.pallas_call(functools.partial(expert_kernel, (experts, ny, nx, slots,...]
    all_gather x1 -> x0, waiting for transfers between devices: 42.8 us -> none  [expert_half(): segment = lax.all_gather(arrived, 'tp', axis=1, tiled=True)]
    reduce_scatter x1 -> x0, waiting for transfers between devices: 37.4 us -> none  [expert_half(): lax.psum_scatter(lax.dot_general(down_block, hidden, (((1,), (1,)), ((),...]
    all_to_all x1 -> x0, blocking collectives: 27.2 us -> none  [expert_half(): lax.all_to_all(outgoing, 'ep', split_axis=0, concat_axis=0, tiled=True)]
    all_to_all x1 -> x0, waiting for transfers between devices: 18.6 us -> none  [expert_half(): lax.all_to_all(results, 'ep', split_axis=1, concat_axis=1, tiled=True)]
    dot_general x4 -> x1, matrix products: 15.5 us -> 0.15 us  [expert_half(): jnp.dot(earlier, visits, preferred_element_type=jnp.float32)]
    gather x2 -> x0, local copies, waits for them, and re-layouts: 4.74 us -> none  [the longest x1 2.68 us: expert_half(): outgoing = narrow[holder].reshape(experts, capacity, column_count)]
    all_to_all x1 -> x0, starting transfers between devices: 4.61 us -> none  [expert_half(): lax.all_to_all(results, 'ep', split_axis=1, concat_axis=1, tiled=True)]
  transfers between devices with their start and end apart: 4 -> 1, of which waited for: 3 -> 0; matrix products, arithmetic and copies ran while one was open for 3% -> 3% of each run, Pallas kernels for 0% -> 84%
where the time goes in v1:
time: 86.9 us; the launch traced here: 85.8 us
  Pallas kernels  72.3 us (83%)
  other arithmetic  7.05 us (8%)
  starting transfers between devices  2.4 us (3%)
  local copies, waits for them, and re-layouts  1.93 us (2%)
  matrix products  1.35 us (2%)
    pallas_call x1, Pallas kernels, expert_half(): pl.pallas_call(functools.partial(expert_kernel, (experts, ny, nx, slots,...  72.3 us
    convert_element_type x1, other arithmetic, rms_rows(): values = row_block.astype(jnp.float32)  2.93 us
    ppermute x1, starting transfers between devices, passed_along(): lax.ppermute(value, axis, [(source, source + steps) for source in range(l...  2.4 us
  transfers between devices with their start and end apart: 1, of which 0 were waited for; matrix products, arithmetic and copies ran while one was open for 3% of the time, Pallas kernels for 84%

profile of v1, /device:TPU:0, one launch (start us, length us, event | category | flops | bytes accessed | tf_op | source)
XLA Modules:
  0.0 85.8 jit_solution(11575461825469108423)
XLA Ops:
  0.6 0.0 copy-start
  0.6 0.0 copy-start.1
  0.7 0.0 copy-start.3
  0.7 0.0 copy-start.4
  0.7 2.9 %convert_element_type.39 = f32[256,2048]{1,0:T(8,128)} convert(bf16[256,2048]{1,0:T(8,128)(2,1)} %param.11) | non-fusion elementwise | flops 524288 | bytes 3145728 | tf_op jit(solution)/shard_map/convert_element_type | solution.py:24
  3.6 0.0 copy-done.1
  3.6 0.3 multiply_reduce_fusion
  3.9 0.8 dynamic-slice
  4.7 1.1 %fusion.8 = bf16[256,512]{1,0:T(8,128)(2,1)S(1)} fusion(f32[256,2048]{1,0:T(8,128)} %convert_element_type.39, s32[]{:T(128)S(6)} %select_n.21, f32[512]{0:T(512)S(1)} %dynamic-slice, f32[256]{0:T(256)S(1)} %add_rsqrt_fusion), kind=kLoop, calls=%fused_computation.24 | loop fusion | flops 393216 | bytes 789508 | tf_op jit(solution)/shard_map/convert_element_type | solution.py:26
  5.9 2.4 %collective-permute-start = (bf16[15,512]{1,0:T(8,128)(2,1)S(1)}, bf16[15,512]{1,0:T(8,128)(2,1)S(1)}, u32[]{:S(2)}, u32[]{:S(2)}) collective-permute-start(bf16[15,512]{1,0:T(8,128)(2,1)S(1)} %slice.24), channel_id=1, source_target_pairs={{0,4},{4,8},{8,12},{12,16},{16,20},{20,24},{24,28},{1,5},{5,9},{9,... | collective-permute-start | bytes 46088 | tf_op jit(solution)/shard_map/ppermute | solution.py:20
  8.3 0.0 copy-done.3
  8.3 0.0 copy-done.4
  8.4 0.1 convolution_convert_fusion
  8.5 0.9 %select_convert_fusion.1.select_ref = bf16[8,96,192]{2,1,0:T(8,128)(2,1)} fusion(bf16[8,192]{1,0:T(8,128)(2,1)S(1)} %bitcast.29, s32[8,192]{1,0:T(8,128)S(1)} %convolution_convert_fusion), kind=kLoop, calls=%fused_computation.10 | loop fusion | flops 294912 | bytes 304128 | tf_op jit(solution)/shard_map/convert_element_type | solution.py:392
  9.4 1.2 %select_convert_fusion.blend_ref = bf16[8,192,96]{2,1,0:T(8,128)(2,1)} fusion(bf16[8,192]{1,0:T(8,128)(2,1)S(1)} %bitcast.28, s32[8,192]{1,0:T(8,128)S(1)} %convolution_convert_fusion), kind=kLoop, calls=%fused_computation.8 | loop fusion | flops 294912 | bytes 304128 | tf_op jit(solution)/shard_map/convert_element_type | solution.py:395
  10.7 72.3 %shard_map.122 = bf16[192,512]{1,0:T(8,128)(2,1)} custom-call(bf16[192,2048]{1,0:T(8,128)(2,1)} %tokens_ref.1, f32[1,2048]{1,0:T(1,128)} %bitcast.30, bf16[8,96,192]{2,1,0:T(8,128)(2,1)} %select_convert_fusion.1.select_ref, bf16[8,192,96]{2,1,0:T(8,128)(2,1)} %select_convert_fusion.blend_ref, bf16[1,2048,1024]{2,1,0:T(8,128)(2,1)} %gate_hbm.1, ...), custom_call_target="tpu_custom_call" | custom-call | tf_op jit(solution)/shard_map/pallas_call | solution.py:403
  82.9 0.0 collective-permute-done
  82.9 0.1 maximum_convert_fusion
  83.0 0.1 pad_add_fusion.2
  83.1 0.1 pad_add_fusion.1
  83.3 0.0 copy-start.5
  83.3 0.1 pad_add_fusion
  83.4 0.1 add_bitcast_fusion
  83.5 0.0 copy-done
  83.5 0.4 copy-done.5
  83.9 0.0 copy-start.2
  83.9 1.2 %fusion = bf16[256,512]{1,0:T(8,128)(2,1)} fusion(bf16[512,512]{1,0:T(8,128)(2,1)S(1)} %copy-done, f32[512]{0:T(512)S(1)} %copy-done.5, bf16[256,512]{1,0:T(8,128)(2,1)S(1)} %fusion.8, s32[]{:T(128)S(6)} %select_n.22, f32[1,271,512]{2,1,0:T(8,128)S(1)} %add_bitcast_fusion, f32[1,271,512]{2,1,0:T(8,128)S(1)} %bitcast.26, f32[1,271,512]{2,1,0:T(8,128)S(1)} %bitcast.25, ...), kind=kOutput, calls=%fused_computation.6 | convolution fusion | flops 135397376 | bytes 3271684 | tf_op jit(solution)/shard_map/dot_general | solution.py:58
  85.1 0.0 copy-done.2
  85.2 0.7 copy.16
  (7 shorter events, 0.1 us)
Async XLA Ops:
  0.6 82.9 %copy-start = (bf16[512,512]{1,0:T(8,128)(2,1)S(1)}, bf16[512,512]{1,0:T(8,128)(2,1)}, u32[]{:S(2)}) copy-start(bf16[512,512]{1,0:T(8,128)(2,1)} %param.13) | copy-start | bytes 1572868
  0.6 3.0 %copy-start.1 = (bf16[256,2048]{1,0:T(8,128)(2,1)S(1)}, bf16[256,2048]{1,0:T(8,128)(2,1)}, u32[]{:S(2)}) copy-start(bf16[256,2048]{1,0:T(8,128)(2,1)} %param.11) | copy-start | bytes 3145732
  0.7 7.6 %copy-start.3 = (f32[192,2]{0,1:T(2,128)S(1)}, f32[192,2]{0,1:T(2,128)}, u32[]{:S(2)}) copy-start(f32[192,2]{0,1:T(2,128)} %param.18) | copy-start | bytes 4612
  0.7 7.7 %copy-start.4 = (s32[192,2]{0,1:T(2,128)S(1)}, s32[192,2]{0,1:T(2,128)}, u32[]{:S(2)}) copy-start(s32[192,2]{0,1:T(2,128)} %param.17) | copy-start | bytes 4612
  5.9 77.0 %collective-permute-start = (bf16[15,512]{1,0:T(8,128)(2,1)S(1)}, bf16[15,512]{1,0:T(8,128)(2,1)S(1)}, u32[]{:S(2)}, u32[]{:S(2)}) collective-permute-start(bf16[15,512]{1,0:T(8,128)(2,1)S(1)} %slice.24), channel_id=1, source_target_pairs={{0,4},{4,8},{8,12},{12,16},{16,20},{20,24},{24,28},{1,5},{5,9},{9,... | collective-permute-start | bytes 46088 | tf_op jit(solution)/shard_map/ppermute | solution.py:20
  83.3 0.7 copy-start.5
  83.9 1.2 %copy-start.2 = (bf16[192,512]{1,0:T(8,128)(2,1)S(1)}, bf16[192,512]{1,0:T(8,128)(2,1)}, u32[]{:S(2)}) copy-start(bf16[192,512]{1,0:T(8,128)(2,1)} %shard_map.122) | copy-start | bytes 589828

commit v2 on v1

--- a/solution.py
+++ b/solution.py
@@ -7,56 +7,8 @@
 from jax.experimental.pallas import tpu as pltpu
 from jax.sharding import PartitionSpec as P
 
-GROUP_WIDTH = 512
-
-
 EPSILON = 1e-06
-halo_rows = 15
-
-
-def passed_along(value, axis, steps):
-    count = lax.axis_size(axis)
-    leading, last = (max(0, -steps), min(count, count - steps))
-    return lax.ppermute(value, axis, [(source, source + steps) for source in range(leading, last)])
-
-
-def rms_rows(row_block, scale_gain):
-    values = row_block.astype(jnp.float32)
-    scaled = values * lax.rsqrt(jnp.mean(values * values, axis=-1, keepdims=True) + EPSILON)
-    return (scaled * scale_gain).astype(jnp.bfloat16)
-
-
-def delayed(values, offset):
-    return jnp.concatenate(
-        [jnp.zeros((offset,) + values.shape[1:], values.dtype), values[:-offset]], axis=0
-    )
-
-
-def window_sums(values):
-    totals = []
-    current = values
-    for offset in (1, 2, 4, 8):
-        current = current + delayed(current, offset)
-        totals.append(current)
-    return totals
-
-
-def pool_half(pool_input, pool_gain, pool_weight, pool_scale):
-    normed = rms_rows(pool_input, pool_gain)
-    local_rows = normed.shape[0]
-    column_count = pool_weight.shape[1]
-    group_index = lax.axis_index("tp") * column_count // GROUP_WIDTH
-    own_group = lax.dynamic_slice_in_dim(normed, group_index * GROUP_WIDTH, GROUP_WIDTH, 1)
-    earlier = passed_along(own_group[local_rows - halo_rows :], "ep", 1)
-    extended = jnp.concatenate([earlier, own_group], axis=0).astype(jnp.float32)
-    stacked = jnp.stack(window_sums(extended))[:, halo_rows:]
-    chosen = lax.dynamic_index_in_dim(stacked, group_index, 0, keepdims=False)
-    position = lax.axis_index("ep") * local_rows + lax.iota(jnp.int32, local_rows)
-    window = jnp.left_shift(jnp.int32(2), group_index)
-    counts = jnp.minimum(position + 1, window).astype(jnp.float32)
-    mixed_in = (chosen / counts[:, None] - own_group.astype(jnp.float32)).astype(jnp.bfloat16)
-    product = jnp.dot(mixed_in, pool_weight, preferred_element_type=jnp.float32)
-    return (product * pool_scale).astype(jnp.bfloat16)
+halo_rows = 16
 
 
 def expert_kernel(
@@ -68,7 +20,12 @@
     gate_hbm,
     up_hbm,
     down_hbm,
+    pool_in_ref,
+    pool_gain_ref,
+    pool_weight_ref,
+    pool_scale_ref,
     out_ref,
+    pool_out_ref,
     normed,
     outgoing,
     sibling_out,
@@ -85,7 +42,11 @@
     gate_ref,
     up_ref,
     down_ref,
+    pool_own,
+    pool_tail,
+    pool_halo,
     weight_sem,
+    halo_sem,
     go_send,
     go_recv,
     a0_send,
@@ -163,10 +124,22 @@
     narrow = normed[:, own_columns]
 
     def pair_at(step):
-        return lax.rem(my_pair + step, pairs)
+        if pairs > 0:
+            return lax.rem(my_pair + step, pairs)
+        flipped, bit = 0, 1
+        while bit < pairs:
+            digit = (my_pair // bit) % 2
+            flipped = flipped + bit * (1 - digit if step & bit else digit)
+            bit *= 2
+        return flipped
+
+    def target_at(step):
+        if pairs > 0:
+            return lax.rem(my_pair + pairs - step, pairs)
+        return pair_at(step)
 
     for step in range(1, pairs):
-        target_pair = lax.rem(my_pair + pairs - step, pairs)
+        target_pair = target_at(step)
         for core in range(2):
             expert = target_pair * 2 + core
             outgoing[expert] = jnp.dot(
@@ -192,7 +165,7 @@
         device_at(sibling, my_y, my_x),
     )
     for step in range(1, pairs):
-        target_pair = lax.rem(my_pair + pairs - step, pairs)
+        target_pair = target_at(step)
         for core in range(2):
             expert = target_pair * 2 + core
             start(
@@ -202,6 +175,44 @@
                 go_recv.at[me],
                 device_at(expert, my_y, my_x),
             )
+
+    group_width = pool_weight_ref.shape[0]
+    group = shard * pool_weight_ref.shape[1] // group_width
+    pool_rows = pool_in_ref.shape[0]
+    halo_count = pool_tail.shape[0]
+
+    def pool_start():
+        inputs = pool_in_ref[...].astype(f32)
+        spread = lax.rsqrt(jnp.mean(inputs * inputs, axis=-1, keepdims=True) + EPSILON)
+        group_columns = pl.ds(pl.multiple_of(group * group_width, group_width), group_width)
+        own = pool_in_ref[:, group_columns].astype(f32)
+        pool_own[...] = (own * spread * pool_gain_ref[:, group_columns]).astype(bf16)
+        pool_tail[...] = pool_own[pool_rows - halo_count :, :]
+        start(
+            pool_tail,
+            pool_halo,
+            halo_sem.at[0],
+            halo_sem.at[1],
+            device_at(lax.rem(me + 1, experts), my_y, my_x),
+        )
+
+    def pool_end():
+        arrive(pool_halo, halo_sem.at[0], halo_sem.at[1])
+        own = pool_own[...].astype(f32)
+        halo = jnp.where(me == 0, 0.0, pool_halo[...].astype(f32))
+        current = jnp.concatenate([halo, own], axis=0)
+        chosen = jnp.zeros_like(current)
+        for number in range(4):
+            current = current + pltpu.roll(current, 1 << number, 0)
+            chosen = jnp.where(group == number, current, chosen)
+        window = jnp.where(group == 0, 2, jnp.where(group == 1, 4, jnp.where(group == 2, 8, 16)))
+        position = me * pool_rows + lax.broadcasted_iota(jnp.int32, (pool_rows, 1), 0)
+        counts = jnp.minimum(position + 1, window).astype(f32)
+        mixed = (chosen[halo_count:] / counts - own).astype(bf16)
+        product = jnp.dot(mixed, pool_weight_ref[...], preferred_element_type=f32)
+        pool_out_ref[...] = (product * pool_scale_ref[...]).astype(bf16)
+
+    sibling_rows = pl.ds(pl.multiple_of((1 - my_core) * slots, slots), slots)
 
     def rows_of(core):
         return pl.ds(core * slots, slots)
@@ -241,6 +252,14 @@
 
     def multiply(step):
         pair = pair_at(step)
+        if step == 0:
+            arrive(
+                rows_in.at[my_pair, :, :, sibling_rows],
+                go_send.at[sibling],
+                go_recv.at[sibling],
+            )
+            for copy in weight_copies:
+                copy.wait()
         entire = jnp.concatenate(
             [rows_in[pair, y, x] for y in range(ny) for x in range(nx)], axis=1
         )
@@ -256,6 +275,9 @@
                     (((1,), (1,)), ((), ())),
                     preferred_element_type=f32,
                 ).astype(bf16)
+
+    def send_parts(step):
+        pair = pair_at(step)
         for x in others_x:
             start(
                 parts.at[pair, :, x, rows_of(0)],
@@ -334,26 +356,22 @@
                 device_at(target, my_y, my_x),
             )
 
-    arrive(
-        rows_in.at[my_pair, :, :, pl.ds(pl.multiple_of((1 - my_core) * slots, slots), slots)],
-        go_send.at[sibling],
-        go_recv.at[sibling],
-    )
-    for copy in weight_copies:
-        copy.wait()
-    multiply(0)
+    schedule = [(multiply, (0,)), (send_parts, (0,)), (pool_start, ())]
     for turn in range(1, pairs + 4):
         if turn < pairs:
-            spread_first(turn)
+            schedule += [(spread_first, (turn,))]
         if 1 <= turn - 1 < pairs:
-            spread_second(turn - 1)
+            schedule += [(spread_second, (turn - 1,))]
+        if turn == 2:
+            schedule += [(pool_end, ())]
         if 1 <= turn - 2 < pairs:
-            spread_end(turn - 2)
-            multiply(turn - 2)
+            schedule += [(spread_end, (turn - 2,)), (multiply, (turn - 2,)), (send_parts, (turn - 2,))]
         if 0 <= turn - 3 < pairs:
-            reduce_first(turn - 3)
+            schedule += [(reduce_first, (turn - 3,))]
         if 0 <= turn - 4 < pairs:
-            reduce_second(turn - 4)
+            schedule += [(reduce_second, (turn - 4,))]
+    for action, arguments in schedule:
+        action(*arguments)
     total = jnp.dot(blend_ref[me], returned[me], preferred_element_type=f32)
     for step in range(1, experts):
         source = lax.rem(me + step, experts)
@@ -364,7 +382,19 @@
         copy.wait_send()
 
 
-def expert_half(moe_input, moe_gain, routes, route_logits, gate_weight, up_weight, down_weight):
+def local(
+    pool_input,
+    pool_gain,
+    pool_weight,
+    pool_scale,
+    moe_input,
+    moe_gain,
+    routes,
+    route_logits,
+    gate_weight,
+    up_weight,
+    down_weight,
+):
     local_rows, row_width = moe_input.shape
     picks_count = routes.shape[1]
     experts, shards = lax.axis_size("ep"), lax.axis_size("tp")
@@ -400,11 +430,14 @@
     anywhere = pl.BlockSpec(memory_space=pl.ANY)
     block = (slots, columns)
     sems_x, sems_y = dma((pairs, nx)), dma((pairs, ny))
-    return pl.pallas_call(
+    expert_out, pool_out = pl.pallas_call(
         functools.partial(expert_kernel, (experts, ny, nx, slots, columns)),
-        out_shape=jax.ShapeDtypeStruct((local_rows, columns), bf16),
-        in_specs=[vmem] * 4 + [anywhere] * 3,
-        out_specs=vmem,
+        out_shape=(
+            jax.ShapeDtypeStruct((local_rows, columns), bf16),
+            jax.ShapeDtypeStruct((pool_input.shape[0], pool_weight.shape[1]), bf16),
+        ),
+        in_specs=[vmem] * 4 + [anywhere] * 3 + [vmem] * 4,
+        out_specs=(vmem, vmem),
         scratch_shapes=[
             pltpu.VMEM((local_rows, row_width), bf16),
             pltpu.VMEM((experts,) + block, bf16),
@@ -422,7 +455,11 @@
             pltpu.VMEM((row_width, hidden_units), bf16),
             pltpu.VMEM((row_width, hidden_units), bf16),
             pltpu.VMEM((row_width, hidden_units), bf16),
+            pltpu.VMEM((pool_input.shape[0], pool_weight.shape[0]), bf16),
+            pltpu.VMEM((halo_rows, pool_weight.shape[0]), bf16),
+            pltpu.VMEM((halo_rows, pool_weight.shape[0]), bf16),
             dma((3,)),
+            dma((2,)),
             dma((experts,)),
             dma((experts,)),
         ]
@@ -439,25 +476,10 @@
         gate_weight,
         up_weight,
         down_weight,
-    )
-
-
-def local(
-    pool_input,
-    pool_gain,
-    pool_weight,
-    pool_scale,
-    moe_input,
-    moe_gain,
-    routes,
-    route_logits,
-    gate_weight,
-    up_weight,
-    down_weight,
-):
-    pool_out = pool_half(pool_input, pool_gain, pool_weight, pool_scale)
-    expert_out = expert_half(
-        moe_input, moe_gain, routes, route_logits, gate_weight, up_weight, down_weight
+        pool_input,
+        pool_gain.reshape(1, row_width),
+        pool_weight,
+        pool_scale.reshape(1, -1),
     )
     return (pool_out, expert_out)
 

time: 86.9 us -> 82.4 us (0.948)
  other arithmetic: 7.05 us -> 4.22 us
  starting transfers between devices: 2.4 us -> 0 us
  Pallas kernels: 72.3 us -> 73.9 us
  local copies, waits for them, and re-layouts: 1.93 us -> 3.29 us
  matrix products: 1.35 us -> 0.15 us
    convert_element_type x6 -> x2, other arithmetic: 6.29 us -> 2.13 us  [the longest x1 1.28 us: local(): blend = jnp.where(rank_of[:, :, None] == slot_ids[None, None, :], share_o...]
    ppermute x1 -> x0, starting transfers between devices: 2.4 us -> none  [passed_along(): lax.ppermute(value, axis, [(source, source + steps) for source in range(l...]
    unnamed x13 -> x2, local copies, waits for them, and re-layouts: 1.12 us -> 3.29 us
    pallas_call x1, Pallas kernels: 72.3 us -> 73.9 us  [local(): pl.pallas_call(functools.partial(expert_kernel, (experts, ny, nx, slots,...]
    dot_general x2 -> x1, matrix products: 1.35 us -> 0.15 us  [local(): jnp.dot(earlier, visits, preferred_element_type=jnp.float32)]
    reduce_sum x3 -> x2, other arithmetic: 0.32 us -> 1.39 us  [the longest x1 0.7 us: local(): shares = raised / jnp.sum(raised, axis=-1, keepdims=True)]
  transfers between devices with their start and end apart: 1 -> 0, of which waited for: 0 -> 0; matrix products, arithmetic and copies ran while one was open for 3% -> 0% of each run, Pallas kernels for 84% -> 0%
where the time goes in v2:
time: 82.4 us; the launch traced here: 82.2 us
  Pallas kernels  73.9 us (90%)
  other arithmetic  4.22 us (5%)
  local copies, waits for them, and re-layouts  3.29 us (4%)
    pallas_call x1, Pallas kernels, local(): pl.pallas_call(functools.partial(expert_kernel, (experts, ny, nx, slots,...  73.9 us
    unnamed x2, local copies, waits for them, and re-layouts  3.29 us

profile of v2, /device:TPU:0, one launch (start us, length us, event | category | flops | bytes accessed | tf_op | source)
XLA Modules:
  0.0 82.2 jit_solution(10376114398615113128)
XLA Ops:
  0.6 0.7 exponential_reduce_fusion
  1.3 0.7 exponential_divide_fusion
  2.0 0.7 select_reduce_fusion
  2.7 0.1 convolution_convert_fusion
  2.9 1.3 %select_convert_fusion.blend_ref = bf16[8,192,96]{2,1,0:T(8,128)(2,1)} fusion(bf16[8,192]{1,0:T(8,128)(2,1)S(1)} %bitcast.7, s32[8,192]{1,0:T(8,128)S(1)} %convolution_convert_fusion), kind=kLoop, calls=%fused_computation.1 | loop fusion | flops 294912 | bytes 304128 | tf_op jit(solution)/shard_map/convert_element_type | solution.py:425
  4.1 0.9 %select_convert_fusion.1.select_ref = bf16[8,96,192]{2,1,0:T(8,128)(2,1)} fusion(bf16[8,192]{1,0:T(8,128)(2,1)S(1)} %bitcast.6, s32[8,192]{1,0:T(8,128)S(1)} %convolution_convert_fusion), kind=kLoop, calls=%fused_computation.3 | loop fusion | flops 294912 | bytes 304128 | tf_op jit(solution)/shard_map/convert_element_type | solution.py:422
  5.0 73.9 %shard_map.122 = (bf16[192,512]{1,0:T(8,128)(2,1)}, bf16[256,512]{1,0:T(8,128)(2,1)}) custom-call(bf16[192,2048]{1,0:T(8,128)(2,1)} %tokens_ref.1, f32[1,2048]{1,0:T(1,128)} %bitcast.8, bf16[8,96,192]{2,1,0:T(8,128)(2,1)} %select_convert_fusion.1.select_ref, bf16[8,192,96]{2,1,0:T(8,128)(2,1)} %select_convert_fusion.blend_ref, ...), custom_call_target="tpu_custom_call" | custom-call | tf_op jit(solution)/shard_map/pallas_call | solution.py:433
  78.9 1.7 %copy.17 = bf16[256,512]{1,0:T(8,128)(2,1)} copy(bf16[256,512]{1,0:T(8,128)(2,1)} %get-tuple-element.10) | data formatting | bytes 524288
  80.6 1.6 %copy.18 = bf16[192,512]{1,0:T(8,128)(2,1)} copy(bf16[192,512]{1,0:T(8,128)(2,1)} %get-tuple-element.11) | data formatting | bytes 393216
